TPU v7x, 32 devices: a whole 2x2x4 slice. The times are simulated.
32 devices in a mesh: ra: 4 (over z), cb: 2 (over y), dp: 4 (over x, core).
Axes of the slice: x: 2, y: 2, z: 4, core: 2. Of those that a mesh axis runs over, the one named last changes fastest.
Arguments:
- stream: bfloat16 [1024, 2048], P('dp', 'ra'), may hold values from -60 to 60
- norm_gain: float32 [2, 2048], P(None, 'ra'), may hold values from 0.1 to 1.9
- gate_weight: float32 [2, 2048, 5504], P(None, 'ra', 'cb'), may hold values from -0.125 to 0.125
- up_weight: float32 [2, 2048, 5504], P(None, 'ra', 'cb'), may hold values from -0.125 to 0.125
- down_weight: float32 [2, 5504, 2048], P(None, 'cb', 'ra'), may hold values from -0.078125 to 0.078125
- gate_scale: float32 [2, 5504], P(None, 'cb'), may hold values from 0.5 to 2
- up_scale: float32 [2, 5504], P(None, 'cb'), may hold values from 0.5 to 2
- down_scale: float32 [2, 2048], P(None, 'ra'), may hold values from 0.5 to 2
Outputs:
- result: bfloat16 [1024, 2048], P('dp', 'ra')
All inputs are finite; a program needn't handle non-finite values.
Results may differ from a plain program's by a relative error of at most 0.04.
Values may be sent and summed in bfloat16 or wider, within the bound.
A program may use at most 128 MiB of HBM per device.

v0:
```python
import jax
import jax.numpy as jnp
from jax import lax
from jax.sharding import PartitionSpec as P

D = 2048


epsilon = 1e-06
residual_scale = 0.5


def activate(gate_part, up_part, squares, gate_scale, up_scale):
    inverse = lax.rsqrt(squares / D + epsilon)
    gate_sum = gate_part * inverse * gate_scale
    up_sum = up_part * inverse * up_scale
    return (jax.nn.silu(gate_sum) * up_sum).astype(jnp.bfloat16)


def half_step(stream, gain, gate_weight, up_weight, down_weight, gate_scale, up_scale, down_scale):
    widened = stream.astype(jnp.float32)
    local_squares = jnp.sum(widened * widened, axis=1, keepdims=True)
    normed = (widened * gain).astype(jnp.bfloat16)
    gate_part = jnp.dot(
        normed, gate_weight.astype(jnp.bfloat16), preferred_element_type=jnp.float32
    ).astype(jnp.bfloat16)
    up_part = jnp.dot(
        normed, up_weight.astype(jnp.bfloat16), preferred_element_type=jnp.float32
    ).astype(jnp.bfloat16)
    total_squares = lax.psum(local_squares, "ra")
    summed = (
        lax.psum_scatter(gate_part, "ra", scatter_dimension=0, tiled=True).astype(jnp.float32),
        lax.psum_scatter(up_part, "ra", scatter_dimension=0, tiled=True).astype(jnp.float32),
    )
    share_rows = summed[0].shape[0]
    squares = lax.dynamic_slice_in_dim(
        total_squares, lax.axis_index("ra") * share_rows, share_rows, 0
    )
    own_hidden = activate(summed[0], summed[1], squares, gate_scale, up_scale)
    hidden = lax.all_gather(own_hidden, "ra", axis=0, tiled=True)
    partial_down = jnp.dot(
        hidden, down_weight.astype(jnp.bfloat16), preferred_element_type=jnp.float32
    )
    branch = lax.psum(partial_down, "cb") * down_scale
    return (residual_scale * widened + branch).astype(jnp.bfloat16)


def on_device(
    stream, norm_gain, gate_weight, up_weight, down_weight, gate_scale, up_scale, down_scale
):
    current = stream
    for block_index in range(2):
        current = half_step(
            current,
            norm_gain[block_index],
            gate_weight[block_index],
            up_weight[block_index],
            down_weight[block_index],
            gate_scale[block_index],
            up_scale[block_index],
            down_scale[block_index],
        )
    return current


def solution(mesh):
    in_specs = (
        P("dp", "ra"),
        P(None, "ra"),
        P(None, "ra", "cb"),
        P(None, "ra", "cb"),
        P(None, "cb", "ra"),
        P(None, "cb"),
        P(None, "cb"),
        P(None, "ra"),
    )
    out_specs = P("dp", "ra")
    return jax.shard_map(
        on_device, mesh=mesh, in_specs=in_specs, out_specs=out_specs, check_vma=False
    )
```

profile of v0, /device:TPU:0, one launch (start us, length us, event | category | flops | bytes accessed | tf_op | source)
XLA Modules:
  0.0 305.1 jit_solution(11187857513949204576)
XLA Ops:
  6.5 0.0 reduce-scatter.5.cloned.1.call-start
  6.5 0.8 fusion.16
  7.3 5.0 %convert.12 = bf16[2,512,2752]{1,2,0:T(8,128)(2,1)S(1)} convert(f32[2,512,2752]{1,2,0:T(8,128)} %param.10) | non-fusion elementwise | flops 2818048 | bytes 16908288 | tf_op jit(solution)/shard_map/convert.5
  12.3 0.0 copy-start.1
  12.3 2.4 copy-done.1
  14.7 2.1 convolution_convert_fusion.3
  16.8 0.0 reduce-scatter.5.cloned.1.call-update
  16.8 0.0 reduce-scatter.7.cloned.1.call-start
  16.8 4.9 %convert.13 = bf16[2,512,2752]{1,2,0:T(8,128)(2,1)S(1)} convert(f32[2,512,2752]{1,2,0:T(8,128)} %param.11) | non-fusion elementwise | flops 2818048 | bytes 16908288 | tf_op jit(solution)/shard_map/convert.4
  21.8 2.5 copy-done
  24.3 2.1 convolution_convert_fusion.2
  26.3 0.0 reduce-scatter.7.cloned.1.call-update
  26.4 0.0 all-gather.3.cloned.1.call-start
  26.4 0.1 fusion.5
  26.5 14.0 %psum.28 = f32[256,1]{0,1:T(1,128)S(1)} all-reduce(f32[256,1]{0,1:T(1,128)S(1)} %bitcast.33), channel_id=1, replica_groups=mesh['ra'=4,'cb'=2,'dp'=4] {'ra'}, use_global_device_ids=true, to_apply=%region_2.0 | all-reduce | flops 256 | bytes 2048 | tf_op jit(solution)/shard_map/psum | solution.py:30
  40.6 0.1 rsqrt_bitcast_fusion.1
  40.6 0.1 slice_reduce_fusion
  40.8 12.6 %reduce-scatter.5.cloned.1.call-done = bf16[64,2752]{1,0:T(8,128)(2,1)} async-done(((bf16[256,2752]{1,0:T(8,128)(2,1)}), bf16[64,2752]{1,0:T(8,128)(2,1)}) %reduce-scatter.5.cloned.1.call-update) | async-done | bytes 352272 | tf_op jit(solution)/shard_map/reduce_scatter | solution.py:32
  53.3 34.5 %reduce-scatter.7.cloned.1.call-done = bf16[64,2752]{1,0:T(8,128)(2,1)} async-done(((bf16[256,2752]{1,0:T(8,128)(2,1)}), bf16[64,2752]{1,0:T(8,128)(2,1)}) %reduce-scatter.7.cloned.1.call-update) | async-done | bytes 352272 | tf_op jit(solution)/shard_map/reduce_scatter | solution.py:33
  87.8 2.2 multiply_convert_fusion.1
  90.0 0.0 all-gather.3.cloned.1.call-update
  90.1 0.0 all-reduce.3.cloned.1.call-start
  90.1 7.4 %convert.14 = bf16[2,2752,512]{2,1,0:T(8,128)(2,1)} convert(f32[2,2752,512]{2,1,0:T(8,128)} %param.12) | non-fusion elementwise | flops 2818048 | bytes 16908288 | tf_op jit(solution)/shard_map/convert.3
  97.5 26.3 %all-gather.3.cloned.1.call-done = bf16[256,2752]{1,0:T(8,128)(2,1)} async-done(((bf16[64,2752]{1,0:T(8,128)(2,1)}), bf16[256,2752]{1,0:T(8,128)(2,1)}) %all-gather.3.cloned.1.call-update) | async-done | bytes 1409040 | tf_op jit(solution)/shard_map/all_gather | solution.py:40
  123.8 4.0 %fusion.1 = f32[256,512]{1,0:T(8,128)} fusion(bf16[256,2752]{1,0:T(8,128)(2,1)} %all-gather.3.cloned.1.call-done, bf16[2,2752,512]{2,1,0:T(8,128)(2,1)} %convert.14), kind=kOutput, calls=%fused_computation.9 | convolution fusion | flops 721420288 | bytes 4784128 | tf_op jit(solution)/shard_map/dot_general | solution.py:41
  127.7 0.0 all-reduce.3.cloned.1.call-update
  127.7 0.0 reduce-scatter.9.cloned.1.call-start
  127.8 0.0 copy-done.5
  127.8 27.7 %all-reduce.3.cloned.1.call-done = f32[256,512]{1,0:T(8,128)} async-done(((f32[256,512]{1,0:T(8,128)}), f32[256,512]{1,0:T(8,128)}) %all-reduce.3.cloned.1.call-update) | async-done | bytes 524304 | tf_op jit(solution)/shard_map/psum | solution.py:44
  155.5 1.2 fusion.9
  156.8 3.9 %convolution_convert_fusion.1 = bf16[256,2752]{1,0:T(8,128)(2,1)} fusion(bf16[2,512,2752]{1,2,0:T(8,128)(2,1)} %copy-done.1, bf16[256,512]{1,0:T(8,128)(2,1)S(1)} %get-tuple-element.10, f32[512]{0:T(512)S(1)} %bitcast.34), kind=kOutput, calls=%fused_computation.1 | convolution fusion | flops 722518016 | bytes 4491264 | tf_op jit(solution)/shard_map/dot_general | solution.py:24
  160.6 0.0 reduce-scatter.9.cloned.1.call-update
  160.6 0.0 reduce-scatter.11.cloned.1.call-start
  160.7 3.9 %convolution_convert_fusion = bf16[256,2752]{1,0:T(8,128)(2,1)} fusion(bf16[2,512,2752]{1,2,0:T(8,128)(2,1)} %copy-done, bf16[256,512]{1,0:T(8,128)(2,1)S(1)} %get-tuple-element.10, f32[512]{0:T(512)S(1)} %bitcast.35), kind=kOutput, calls=%fused_computation | convolution fusion | flops 722518016 | bytes 4491264 | tf_op jit(solution)/shard_map/dot_general | solution.py:27
  164.6 0.0 reduce-scatter.11.cloned.1.call-update
  164.6 0.0 all-gather.5.cloned.1.call-start
  164.7 12.3 %psum.30 = f32[256,1]{0,1:T(1,128)S(1)} all-reduce(f32[256,1]{0,1:T(1,128)S(1)} %bitcast.32), channel_id=1, replica_groups=mesh['ra'=4,'cb'=2,'dp'=4] {'ra'}, use_global_device_ids=true, to_apply=%region_7.8 | all-reduce | flops 256 | bytes 2048 | tf_op jit(solution)/shard_map/psum | solution.py:30
  176.9 0.1 rsqrt_bitcast_fusion
  177.0 17.4 %reduce-scatter.9.cloned.1.call-done = bf16[64,2752]{1,0:T(8,128)(2,1)} async-done(((bf16[256,2752]{1,0:T(8,128)(2,1)}), bf16[64,2752]{1,0:T(8,128)(2,1)}) %reduce-scatter.9.cloned.1.call-update) | async-done | bytes 352272 | tf_op jit(solution)/shard_map/reduce_scatter | solution.py:32
  194.4 34.4 %reduce-scatter.11.cloned.1.call-done = bf16[64,2752]{1,0:T(8,128)(2,1)} async-done(((bf16[256,2752]{1,0:T(8,128)(2,1)}), bf16[64,2752]{1,0:T(8,128)(2,1)}) %reduce-scatter.11.cloned.1.call-update) | async-done | bytes 352272 | tf_op jit(solution)/shard_map/reduce_scatter | solution.py:33
  228.8 2.2 multiply_convert_fusion
  231.0 0.0 all-gather.5.cloned.1.call-update
  231.0 0.0 all-reduce.5.cloned.1.call-start
  231.1 33.6 %all-gather.5.cloned.1.call-done = bf16[256,2752]{1,0:T(8,128)(2,1)} async-done(((bf16[64,2752]{1,0:T(8,128)(2,1)}), bf16[256,2752]{1,0:T(8,128)(2,1)}) %all-gather.5.cloned.1.call-update) | async-done | bytes 1409040 | tf_op jit(solution)/shard_map/all_gather | solution.py:40
  264.7 3.9 %fusion = f32[256,512]{1,0:T(8,128)} fusion(bf16[256,2752]{1,0:T(8,128)(2,1)} %all-gather.5.cloned.1.call-done, bf16[2,2752,512]{2,1,0:T(8,128)(2,1)} %convert.14), kind=kOutput, calls=%fused_computation.5 | convolution fusion | flops 721420288 | bytes 4784128 | tf_op jit(solution)/shard_map/dot_general | solution.py:41
  268.6 0.0 all-reduce.5.cloned.1.call-update
  268.7 27.8 %all-reduce.5.cloned.1.call-done = f32[256,512]{1,0:T(8,128)} async-done(((f32[256,512]{1,0:T(8,128)}), f32[256,512]{1,0:T(8,128)}) %all-reduce.5.cloned.1.call-update) | async-done | bytes 524304 | tf_op jit(solution)/shard_map/psum | solution.py:44
  296.4 1.8 fusion.7
  (9 shorter events, 0.0 us)
Async XLA Ops:
  6.5 46.8 %reduce-scatter.5.cloned.1.call-start = ((), (), s32[]{:S(2)}) async-start(), calls=%async_computation.4 | async-start | bytes 1802240 | tf_op jit(solution)/shard_map/reduce_scatter | solution.py:32
  7.3 7.4 %copy-start.2 = (bf16[256,512]{1,0:T(8,128)(2,1)S(1)}, bf16[256,512]{1,0:T(8,128)(2,1)}, u32[]{:S(2)}) copy-start(bf16[256,512]{1,0:T(8,128)(2,1)} %param.8) | copy-start | bytes 786436
  12.3 2.4 copy-start.1
  16.8 71.1 %reduce-scatter.7.cloned.1.call-start = ((), (), s32[]{:S(2)}) async-start(), calls=%async_computation.5 | async-start | bytes 1802240 | tf_op jit(solution)/shard_map/reduce_scatter | solution.py:33
  21.8 2.5 copy-start
  24.3 16.4 %copy-start.3 = (f32[2,2752]{1,0:T(2,128)S(1)}, f32[2,2752]{1,0:T(2,128)}, u32[]{:S(2)}) copy-start(f32[2,2752]{1,0:T(2,128)} %param.14) | copy-start | bytes 66052
  24.3 16.4 %copy-start.4 = (f32[2,2752]{1,0:T(2,128)S(1)}, f32[2,2752]{1,0:T(2,128)}, u32[]{:S(2)}) copy-start(f32[2,2752]{1,0:T(2,128)} %param.13) | copy-start | bytes 66052
  26.4 97.4 %all-gather.3.cloned.1.call-start = ((), (), s32[]{:S(2)}) async-start(), calls=%async_computation.6 | async-start | bytes 1802240 | tf_op jit(solution)/shard_map/all_gather | solution.py:40
  90.1 65.5 %all-reduce.3.cloned.1.call-start = ((), (), s32[]{:S(2)}) async-start(), calls=%async_computation.7 | async-start | bytes 1048576 | tf_op jit(solution)/shard_map/psum | solution.py:44
  97.5 30.3 %copy-start.5 = (f32[2,512]{1,0:T(2,128)S(1)}, f32[2,512]{1,0:T(2,128)}, u32[]{:S(2)}) copy-start(f32[2,512]{1,0:T(2,128)} %param.15) | copy-start | bytes 12292
  127.7 66.6 %reduce-scatter.9.cloned.1.call-start = ((), (), s32[]{:S(2)}) async-start(), calls=%async_computation.8 | async-start | bytes 1802240 | tf_op jit(solution)/shard_map/reduce_scatter | solution.py:32
  160.6 68.1 %reduce-scatter.11.cloned.1.call-start = ((), (), s32[]{:S(2)}) async-start(), calls=%async_computation.9 | async-start | bytes 1802240 | tf_op jit(solution)/shard_map/reduce_scatter | solution.py:33
  164.6 100.1 %all-gather.5.cloned.1.call-start = ((), (), s32[]{:S(2)}) async-start(), calls=%async_computation.10 | async-start | bytes 1802240 | tf_op jit(solution)/shard_map/all_gather | solution.py:40
  231.0 65.4 %all-reduce.5.cloned.1.call-start = ((), (), s32[]{:S(2)}) async-start(), calls=%async_computation.11 | async-start | bytes 1048576 | tf_op jit(solution)/shard_map/psum | solution.py:44
Sparse Core Ops, SparseCore 0:
  16.9 36.3 reduce-scatter.4
  55.6 32.1 reduce-scatter.6
  90.2 33.5 all-gather.2
  127.9 27.6 all-reduce.2
  160.8 33.5 reduce-scatter.8
  196.5 32.2 reduce-scatter.10
  231.1 33.5 all-gather.4
  268.8 27.6 all-reduce.4
where the time goes:
time: 306 us; the launch traced here: 305 us
  waiting for transfers between devices  214 us (70%)
  blocking collectives  26.3 us (9%)
  other arithmetic  25 us (8%)
  matrix products  19.8 us (6%)
  between operations  13.6 us (4%)
  local copies, waits for them, and re-layouts  5.78 us (2%)
    reduce_scatter x2, waiting for transfers between devices, half_step(): lax.psum_scatter(up_part, 'ra', scatter_dimension=0, tiled=True)  68.9 us
    all_gather x2, waiting for transfers between devices, half_step(): hidden = lax.all_gather(own_hidden, 'ra', axis=0, tiled=True)  59.9 us
    psum x2, waiting for transfers between devices, half_step(): branch = lax.psum(partial_down, 'cb') * down_scale  55.5 us
    reduce_scatter x2, waiting for transfers between devices, half_step(): lax.psum_scatter(gate_part, 'ra', scatter_dimension=0, tiled=True)  29.9 us
    psum x2, blocking collectives, half_step(): total_squares = lax.psum(local_squares, 'ra')  26.3 us
    another operation x3, other arithmetic  17.3 us
    dot_general x2, matrix products, half_step(): jnp.dot(hidden, down_weight.astype(jnp.bfloat16), preferred_element_type=...  7.9 us
  transfers between devices with their start and end apart: 8, of which 8 were waited for; matrix products, arithmetic and copies ran while one was open for 6% of the time, Pallas kernels for 0%

commit v1 on v0

v1 whole, which is shorter than its diff:
```python
import functools

import jax
import jax.numpy as jnp
from jax import lax
from jax.experimental import pallas as pl
from jax.experimental.pallas import tpu as pltpu
from jax.sharding import PartitionSpec as P

MESH = pl.DeviceIdType.MESH
epsilon = 1e-06
residual_scale = 0.5
WIDTH = 128
TILE = 256
LAG = 2
SUBLANES = 8


def kernel(
    n, m, stream, gain, gate_hbm, up_hbm, down_hbm, gate_scale, up_scale, down_scale, out,
    gate_v, up_v, down_v, part, sums_in, hidden, sq, sq_in, inverse, scales, normed, acc, y_buf, current,
    w_sem, rs_send, rs_recv, ag_send, ag_recv, sq_send, sq_recv, y_send, y_recv,
):
    blocks = gate_hbm.shape[0]
    units = gate_hbm.shape[2]
    rows, depth = stream.shape
    half = rows // 2
    features = depth * n
    chunks = pl.cdiv(units, WIDTH)
    r = lax.axis_index("ra")
    q = lax.axis_index("cb")
    first, final = r == 0, r == n - 1
    left, right = jnp.maximum(r - 1, 0), jnp.minimum(r + 1, n - 1)
    head, last = (final, first), (first, final)
    onward, back = (left, right), (right, left)
    passed = (n - 1 - r, r)

    def weight_copies(b):
        return [
            pltpu.make_async_copy(hbm.at[b], vmem.at[b], w_sem.at[b, i])
            for i, (hbm, vmem) in enumerate(
                ((gate_hbm, gate_v), (up_hbm, up_v), (down_hbm, down_v))
            )
        ]

    loads = [weight_copies(b) for b in range(blocks)]
    loads[0][0].start()
    loads[0][1].start()

    barrier = pltpu.get_barrier_semaphore()

    for i in range(1, n):
        peer = lax.rem(r + i, n)
        pl.semaphore_signal(barrier, inc=1, device_id={"ra": peer}, device_id_type=MESH)

    for i in range(1, m):
        peer = lax.rem(q + i, m)
        pl.semaphore_signal(barrier, inc=1, device_id={"cb": peer}, device_id_type=MESH)

    def sum_copy(b, d, c):
        return pltpu.make_async_remote_copy(
            src_ref=part.at[b, c, d], dst_ref=sums_in.at[b, c, d],
            send_sem=rs_send.at[b, d, c], recv_sem=rs_recv.at[b, d, c],
            device_id={"ra": onward[d]}, device_id_type=MESH,
        )

    def hidden_copy(b, d, c):
        piece = hidden.at[b, c, pl.ds(d * half, half)]
        return pltpu.make_async_remote_copy(
            src_ref=piece, dst_ref=piece,
            send_sem=ag_send.at[b, d, c], recv_sem=ag_recv.at[b, d, c],
            device_id={"ra": back[d]}, device_id_type=MESH,
        )

    def squares_copy(b, d, source):
        return pltpu.make_async_remote_copy(
            src_ref=sq.at[b, d], dst_ref=sq_in.at[b, d, source],
            send_sem=sq_send.at[b, d], recv_sem=sq_recv.at[b, d, source],
            device_id={"ra": (n - 1) * d}, device_id_type=MESH,
        )

    def branch_copy(b, i):
        return pltpu.make_async_remote_copy(
            src_ref=y_buf.at[b, q], dst_ref=y_buf.at[b, q],
            send_sem=y_send.at[b, i - 1], recv_sem=y_recv.at[b, q],
            device_id={"cb": lax.rem(q + i, m)}, device_id_type=MESH,
        )

    def branch_arrival(b, i):
        source = lax.rem(q + i, m)
        return pltpu.make_async_remote_copy(
            src_ref=y_buf.at[b, source], dst_ref=y_buf.at[b, source],
            send_sem=y_send.at[b, i - 1], recv_sem=y_recv.at[b, source],
            device_id={"cb": source}, device_id_type=MESH,
        )

    current[...] = stream[...]
    for c in range(chunks):
        lo = c * WIDTH
        w = min(WIDTH, units - lo)
        for b in range(blocks):
            for g, scale in enumerate((gate_scale, up_scale)):
                scales[g, b, c, :, :w] = scale[b : b + 1, lo : lo + w]

    for b in range(blocks):
        widened = current[...].astype(jnp.float32)
        normed[...] = (widened * gain[b : b + 1, :]).astype(jnp.bfloat16)
        squares = jnp.sum(widened * widened, axis=1, keepdims=True)
        for d in range(2):
            column = squares[d * half : (d + 1) * half]
            sq[b, d] = jnp.broadcast_to(column, (half, WIDTH)).T[:SUBLANES]

        if b == 0:
            pl.semaphore_wait(barrier, n - 1 + m - 1)

        for d in range(2):
            @pl.when(jnp.logical_not(last[d]))
            def _(d=d):
                squares_copy(b, d, r).start()

        loads[b][0].wait()
        loads[b][1].wait()
        if b == 0:
            loads[0][2].start()
            for later in range(1, blocks):
                for load in loads[later]:
                    load.start()

        for lo in range(0, units, TILE):
            w = min(TILE, units - lo)
            cuts = [(at, min(WIDTH, w - at)) for at in range(0, w, WIDTH)]
            for g, weight in enumerate((gate_v, up_v)):
                piece = jnp.dot(
                    normed[...], weight[b, :, lo : lo + w].astype(jnp.bfloat16),
                    preferred_element_type=jnp.float32,
                ).astype(jnp.bfloat16)
                for d in range(2):
                    for at, cut in cuts:
                        part[b, (lo + at) // WIDTH, d, g, :, :cut] = piece[
                            d * half : (d + 1) * half, at : at + cut
                        ]
            for d in range(2):
                @pl.when(head[d])
                def _(d=d, lo=lo, cuts=cuts):
                    for at, cut in cuts:
                        sum_copy(b, d, (lo + at) // WIDTH).start()

        loads[b][2].wait()
        acc[...] = jnp.zeros_like(acc)
        pairs = units // TILE

        def step(t, carry, b=b):
            for d in range(2):
                c = t - (passed[d] - 1) * LAG
                live = (passed[d] > 0) & (c >= 0) & (c < chunks)

                @pl.when(live & jnp.logical_not(last[d]))
                def _(d=d, c=c):
                    sum_copy(b, d, c).wait_recv()
                    part[b, c, d] = (
                        part[b, c, d].astype(jnp.float32) + sums_in[b, c, d].astype(jnp.float32)
                    ).astype(jnp.bfloat16)
                    sum_copy(b, d, c).start()

                @pl.when(live & last[d] & (c == 0))
                def _(d=d):
                    total = sq[b, d]
                    for i in range(1, n):
                        source = lax.rem(r + i, n)
                        squares_copy(b, d, source).wait_recv()
                        total = total + sq_in[b, d, source]
                    column = jnp.broadcast_to(total[:1], (WIDTH, half)).T
                    inverse[b, d] = lax.rsqrt(column / features + epsilon)

                @pl.when(live & last[d])
                def _(d=d, c=c):
                    sum_copy(b, d, c).wait_recv()
                    gate_sum, up_sum = (
                        (
                            part[b, c, d, g].astype(jnp.float32)
                            + sums_in[b, c, d, g].astype(jnp.float32)
                        )
                        * inverse[b, d]
                        * scales[g, b, c]
                        for g in range(2)
                    )
                    active = gate_sum / (1.0 + jnp.exp(-gate_sum)) * up_sum
                    hidden[b, c, d * half : (d + 1) * half, :] = active.astype(jnp.bfloat16)
                    hidden_copy(b, d, c).start()

            for d in range(2):
                far = n - 1 - passed[d]
                c = t - (n - 2 + far) * LAG
                live = (far > 0) & (c >= 0) & (c < chunks)

                @pl.when(live)
                def _(d=d, c=c):
                    hidden_copy(b, d, c).wait_recv()

                @pl.when(live & jnp.logical_not(head[d]))
                def _(d=d, c=c):
                    hidden_copy(b, d, c).start()

            c = t - (2 * n - 3) * LAG

            @pl.when((c >= 0) & (lax.rem(c, 2) == 1) & (c < 2 * pairs))
            def _():
                both = jnp.concatenate([hidden[b, c - 1], hidden[b, c]], axis=1)
                at = pl.multiple_of((c - 1) * WIDTH, TILE)
                acc[...] += jnp.dot(
                    both, down_v[b, pl.ds(at, TILE), :].astype(jnp.bfloat16),
                    preferred_element_type=jnp.float32,
                )

            return carry

        lax.fori_loop(0, chunks + (2 * n - 3) * LAG, step, 0)
        for c in range(2 * pairs, chunks):
            lo = c * WIDTH
            w = min(WIDTH, units - lo)
            acc[...] += jnp.dot(
                hidden[b, c, :, :w], down_v[b, lo : lo + w, :].astype(jnp.bfloat16),
                preferred_element_type=jnp.float32,
            )

        y_buf[b, q] = acc[...].astype(jnp.bfloat16)
        for i in range(1, m):
            branch_copy(b, i).start()
        for i in range(1, m):
            branch_arrival(b, i).wait_recv()
        branch = y_buf[b, 0].astype(jnp.float32)
        for j in range(1, m):
            branch = branch + y_buf[b, j].astype(jnp.float32)
        branch = branch * down_scale[b : b + 1, :]
        result = (residual_scale * current[...].astype(jnp.float32) + branch).astype(jnp.bfloat16)
        if b == blocks - 1:
            out[...] = result
        else:
            current[...] = result

    for b in range(blocks):
        for i in range(1, m):
            branch_copy(b, i).wait_send()
        for d in range(2):
            @pl.when(jnp.logical_not(last[d]))
            def _(d=d, b=b):
                squares_copy(b, d, r).wait_send()

                @pl.loop(0, chunks)
                def _(c):
                    sum_copy(b, d, c).wait_send()

            @pl.when(jnp.logical_not(head[d]))
            def _(d=d, b=b):
                @pl.loop(0, chunks)
                def _(c):
                    hidden_copy(b, d, c).wait_send()


def on_device(n, m, stream, norm_gain, gate_weight, up_weight, down_weight, gate_scale, up_scale, down_scale):
    rows, depth = stream.shape
    half = rows // 2
    blocks, _, units = gate_weight.shape
    chunks = pl.cdiv(units, WIDTH)
    vmem = pl.BlockSpec(memory_space=pltpu.VMEM)
    whole = pl.BlockSpec(memory_space=pl.ANY)
    dma = pltpu.SemaphoreType.DMA
    return pl.pallas_call(
        functools.partial(kernel, n, m),
        out_shape=jax.ShapeDtypeStruct(stream.shape, jnp.bfloat16),
        in_specs=[vmem, vmem, whole, whole, whole, vmem, vmem, vmem],
        out_specs=vmem,
        scratch_shapes=[
            pltpu.VMEM(gate_weight.shape, jnp.float32),
            pltpu.VMEM(up_weight.shape, jnp.float32),
            pltpu.VMEM(down_weight.shape, jnp.float32),
            pltpu.VMEM((blocks, chunks, 2, 2, half, WIDTH), jnp.bfloat16),
            pltpu.VMEM((blocks, chunks, 2, 2, half, WIDTH), jnp.bfloat16),
            pltpu.VMEM((blocks, chunks, rows, WIDTH), jnp.bfloat16),
            pltpu.VMEM((blocks, 2, SUBLANES, half), jnp.float32),
            pltpu.VMEM((blocks, 2, n, SUBLANES, half), jnp.float32),
            pltpu.VMEM((blocks, 2, half, WIDTH), jnp.float32),
            pltpu.VMEM((2, blocks, chunks, 1, WIDTH), jnp.float32),
            pltpu.VMEM((rows, depth), jnp.bfloat16),
            pltpu.VMEM((rows, depth), jnp.float32),
            pltpu.VMEM((blocks, m, rows, depth), jnp.bfloat16),
            pltpu.VMEM((rows, depth), jnp.bfloat16),
            dma((blocks, 3)),
            dma((blocks, 2, chunks)),
            dma((blocks, 2, chunks)),
            dma((blocks, 2, chunks)),
            dma((blocks, 2, chunks)),
            dma((blocks, 2)),
            dma((blocks, 2, n)),
            dma((blocks, m)),
            dma((blocks, m)),
        ],
        compiler_params=pltpu.CompilerParams(
            collective_id=0, has_side_effects=True, vmem_limit_bytes=67043328
        ),
    )(stream, norm_gain, gate_weight, up_weight, down_weight, gate_scale, up_scale, down_scale)


def solution(mesh):
    in_specs = (
        P("dp", "ra"),
        P(None, "ra"),
        P(None, "ra", "cb"),
        P(None, "ra", "cb"),
        P(None, "cb", "ra"),
        P(None, "cb"),
        P(None, "cb"),
        P(None, "ra"),
    )
    return jax.shard_map(
        functools.partial(on_device, mesh.shape["ra"], mesh.shape["cb"]),
        mesh=mesh, in_specs=in_specs, out_specs=P("dp", "ra"), check_vma=False,
    )
```

time: 306 us -> 202 us (0.66)
  waiting for transfers between devices: 214 us -> 0 us
  Pallas kernels: 0 us -> 176 us
  blocking collectives: 26.3 us -> 0 us
  other arithmetic: 25 us -> 0 us
  matrix products: 19.8 us -> 0 us
  local copies, waits for them, and re-layouts: 5.78 us -> 25.5 us
  between operations: 13.6 us -> 0.01 us
    pallas_call x0 -> x1, Pallas kernels: none -> 176 us  [on_device(): pl.pallas_call(functools.partial(kernel, n, m), out_shape=jax.ShapeDtypeS...]
    reduce_scatter x4 -> x0, waiting for transfers between devices: 98.9 us -> none  [the longest x2 68.9 us: half_step(): lax.psum_scatter(up_part, 'ra', scatter_dimension=0, tiled=True)]
    all_gather x2 -> x0, waiting for transfers between devices: 59.9 us -> none  [half_step(): hidden = lax.all_gather(own_hidden, 'ra', axis=0, tiled=True)]
    psum x2 -> x0, waiting for transfers between devices: 55.5 us -> none  [half_step(): branch = lax.psum(partial_down, 'cb') * down_scale]
    psum x2 -> x0, blocking collectives: 26.3 us -> none  [half_step(): total_squares = lax.psum(local_squares, 'ra')]
    unnamed x12 -> x3, local copies, waits for them, and re-layouts: 4.89 us -> 25.5 us
    dot_general x6 -> x0, matrix products: 19.8 us -> none  [the longest x2 7.9 us: half_step(): jnp.dot(hidden, down_weight.astype(jnp.bfloat16), preferred_element_type=...]
    another operation x3 -> x0, other arithmetic: 17.3 us -> none
  transfers between devices with their start and end apart: 8 -> 0, of which waited for: 8 -> 0; matrix products, arithmetic and copies ran while one was open for 6% -> 0% of each run, Pallas kernels for 0% -> 0%
where the time goes in v1:
time: 202 us; the launch traced here: 201 us
  Pallas kernels  176 us (87%)
  local copies, waits for them, and re-layouts  25.5 us (13%)
    pallas_call x1, Pallas kernels, on_device(): pl.pallas_call(functools.partial(kernel, n, m), out_shape=jax.ShapeDtypeS...  176 us
    unnamed x3, local copies, waits for them, and re-layouts  25.5 us

profile of v1, /device:TPU:0, one launch (start us, length us, event | category | flops | bytes accessed | tf_op | source)
XLA Modules:
  0.0 201.4 jit_solution(14665709470854143893)
XLA Ops:
  0.0 12.0 %copy.9.gate_hbm = f32[2,512,2752]{2,1,0:T(8,128)} copy(f32[2,512,2752]{1,2,0:T(8,128)} %param.10) | data formatting | bytes 22544384 | tf_op args[2]
  12.0 11.9 %copy.10.up_hbm = f32[2,512,2752]{2,1,0:T(8,128)} copy(f32[2,512,2752]{1,2,0:T(8,128)} %param.11) | data formatting | bytes 22544384 | tf_op args[3]
  23.9 175.9 %shard_map.82 = bf16[256,512]{1,0:T(8,128)(2,1)} custom-call(bf16[256,512]{1,0:T(8,128)(2,1)} %stream.1, f32[2,512]{1,0:T(2,128)} %gain.1, f32[2,512,2752]{2,1,0:T(8,128)} %copy.9.gate_hbm, f32[2,512,2752]{2,1,0:T(8,128)} %copy.10.up_hbm, f32[2,2752,512]{2,1,0:T(8,128)} %down_hbm.1, f32[2,2752]{1,0:T(2,128)} %gate_scale.1, f32[2,2752]{1,0:T(2,128)} %up_scale.1, ...), custom_call_target="tpu_custom_call" | custom-call | tf_op jit(solution)/shard_map/pallas_call | solution.py:268
  199.7 1.7 copy.12

commit v2 on v1

--- a/solution.py
+++ b/solution.py
@@ -12,6 +12,7 @@
 residual_scale = 0.5
 WIDTH = 128
 TILE = 256
+AHEAD = 4
 LAG = 2
 SUBLANES = 8
 
@@ -143,13 +144,19 @@
                 @pl.when(head[d])
                 def _(d=d, lo=lo, cuts=cuts):
                     for at, cut in cuts:
-                        sum_copy(b, d, (lo + at) // WIDTH).start()
+                        if (lo + at) // WIDTH < AHEAD:
+                            sum_copy(b, d, (lo + at) // WIDTH).start()
 
         loads[b][2].wait()
         acc[...] = jnp.zeros_like(acc)
         pairs = units // TILE
 
         def step(t, carry, b=b):
+            for d in range(2):
+                @pl.when(head[d] & (t + AHEAD < chunks))
+                def _(d=d):
+                    sum_copy(b, d, t + AHEAD).start()
+
             for d in range(2):
                 c = t - (passed[d] - 1) * LAG
                 live = (passed[d] > 0) & (c >= 0) & (c < chunks)

time: 202 us -> 174 us (0.86)
  Pallas kernels: 176 us -> 148 us
    pallas_call x1, Pallas kernels: 176 us -> 148 us  [on_device(): pl.pallas_call(functools.partial(kernel, n, m), out_shape=jax.ShapeDtypeS...]
where the time goes in v2:
time: 174 us
  Pallas kernels  148 us (85%)
  local copies, waits for them, and re-layouts  25.5 us (15%)
    pallas_call x1, Pallas kernels, on_device(): pl.pallas_call(functools.partial(kernel, n, m), out_shape=jax.ShapeDtypeS...  148 us
    unnamed x3, local copies, waits for them, and re-layouts  25.5 us

profile of v2, /device:TPU:0, one launch (start us, length us, event | category | flops | bytes accessed | tf_op | source)
XLA Modules:
  0.0 173.6 jit_solution(12961091157376686994)
XLA Ops:
  0.0 12.0 %copy.9.gate_hbm = f32[2,512,2752]{2,1,0:T(8,128)} copy(f32[2,512,2752]{1,2,0:T(8,128)} %param.10) | data formatting | bytes 22544384 | tf_op args[2]
  12.0 11.9 %copy.10.up_hbm = f32[2,512,2752]{2,1,0:T(8,128)} copy(f32[2,512,2752]{1,2,0:T(8,128)} %param.11) | data formatting | bytes 22544384 | tf_op args[3]
  23.9 148.0 %shard_map.82 = bf16[256,512]{1,0:T(8,128)(2,1)} custom-call(bf16[256,512]{1,0:T(8,128)(2,1)} %stream.1, f32[2,512]{1,0:T(2,128)} %gain.1, f32[2,512,2752]{2,1,0:T(8,128)} %copy.9.gate_hbm, f32[2,512,2752]{2,1,0:T(8,128)} %copy.10.up_hbm, f32[2,2752,512]{2,1,0:T(8,128)} %down_hbm.1, f32[2,2752]{1,0:T(2,128)} %gate_scale.1, f32[2,2752]{1,0:T(2,128)} %up_scale.1, ...), custom_call_target="tpu_custom_call" | custom-call | tf_op jit(solution)/shard_map/pallas_call | solution.py:275
  171.9 1.7 copy.12
